TPU v7x, 128 devices: a whole 4x4x4 slice. The times are simulated.
128 devices in a mesh: sp: 16 (over z, x), tp: 8 (over y, core).
Axes of the slice: x: 4, y: 4, z: 4, core: 2. Of those that a mesh axis runs over, the one named last changes fastest.
Arguments:
- residual: bfloat16 [8192, 4096], P('sp'), may hold values from -6 to 6
- queries: bfloat16 [8192, 1024], P('sp', 'tp'), may hold values from -6 to 6
- projected_key_rows: bfloat16 [8192, 1024], P('sp', 'tp'), may hold values from -6 to 6
- projected_value_rows: bfloat16 [8192, 2048], P('sp', 'tp'), may hold values from -6 to 6
- output_gate_logits: bfloat16 [8192, 2048], P('sp', 'tp'), may hold values from -6 to 6
- input_gate_logits: float32 [16, 8192], P('tp', 'sp'), may hold values from -8 to 120
- forget_gate_logits: float32 [16, 8192], P('tp', 'sp'), may hold values from 0 to 16
- extra_forget_logits: float32 [16, 8192], P('tp', 'sp'), may hold values from -0.7 to 0, as said below
- head_norm_gain: bfloat16 [2048], P('tp'), may hold values from 0.099609375 to 1.8984375
- output_projection_weight: bfloat16 [2048, 4096], P('tp'), may hold values from -0.125 to 0.125
- feedforward_norm_gain: bfloat16 [4096], replicated, may hold values from 0.099609375 to 1.8984375
- feedforward_gate_weight: bfloat16 [4096, 11264], P('sp', 'tp'), may hold values from -0.09375 to 0.09375
- up_projection_weight: bfloat16 [4096, 11264], P('sp', 'tp'), may hold values from -0.09375 to 0.09375
- down_projection_weight: bfloat16 [4096, 11264], P('sp', 'tp'), may hold values from -0.0546875 to 0.0546875
Outputs:
- layer_out: bfloat16 [8192, 4096], P(('sp', 'tp'))
Inputs may be any that keep to these rules, and one draw needn't show every extreme that they name: `extra_forget_logits`: each entry is 0 or the logarithm of a factor between one half and 0.8.
All inputs are finite; a program needn't handle non-finite values.
Results may differ from a plain program's by a relative error of at most 0.01.
Values may be sent and summed in bfloat16 or wider, within the bound.
A program may use at most 192 MiB of HBM per device.

v0:
```python
import jax
import jax.numpy as jnp
from jax import lax
from jax.sharding import Mesh
from jax.sharding import PartitionSpec as P

QK_DIM = 64
V_DIM = 128
BLOCK = 64
TP = ("tp_0", "tp_1")
SP_TP = ("sp", "tp_0", "tp_1")


def sent_together(arrays, axis, dim, along):
    both = jnp.concatenate(arrays, axis=along)
    out, at, outs = (lax.all_gather(both, axis, axis=dim, tiled=True), 0, [])
    for a in arrays:
        outs.append(lax.slice_in_dim(out, at, at + a.shape[along], axis=along))
        at += a.shape[along]
    return tuple(outs)


def sent_to_all(shard, axis):
    count = lax.axis_size(axis)
    return lax.all_to_all(
        jnp.broadcast_to(shard[None], (count, *shard.shape)), axis, 0, 0, tiled=True
    )


def all_in_one(shard, axis):
    leaves = jax.tree.leaves(shard)
    order = sorted(range(len(leaves)), key=lambda k: -leaves[k].size)
    width = (1, *leaves[order[0]].shape)[-1]
    lines = [
        jnp.pad(leaves[k].reshape(-1), (0, -leaves[k].size % width)).reshape(-1, width)
        for k in order
    ]
    both, at, found = (sent_to_all(jnp.concatenate(lines), axis), 0, {})
    for k, line in zip(order, lines):
        share = both[:, at : at + len(line)].reshape(len(both), -1)
        found[k] = share[:, : leaves[k].size].reshape(-1, *leaves[k].shape)
        at += len(line)
    numbers = iter(range(len(leaves)))
    return jax.tree.map(lambda _: found[next(numbers)], shard)


def folded_in_pairs(pieces, combine):
    while len(jax.tree.leaves(pieces)[0]) > 1:
        pieces = jax.vmap(combine)(
            *(jax.tree.map(lambda part: part[side::2], pieces) for side in (0, 1))
        )
    return jax.tree.map(lambda part: part[0], pieces)


def carried_in(shard, axis, combine, identity):
    count, index = (lax.axis_size(axis), lax.axis_index(axis))
    passed = jnp.arange(count) < index

    def kept(part, zero, own):
        part = jnp.where(
            passed.reshape(-1, *(1 for _ in own.shape)), part, jnp.asarray(zero, own.dtype)
        )
        return part

    pieces = all_in_one(shard, axis)
    return folded_in_pairs(jax.tree.map(kept, pieces, identity, shard), combine)


def split_up(shard, dim, count):
    lengths = shard.shape
    pieces = shard.reshape(*lengths[:dim], count, lengths[dim] // count, *lengths[dim + 1 :])
    return jnp.moveaxis(pieces, dim, 0)


def summed_on_arrival(shard, axis, dim):
    count = lax.axis_size(axis)
    pieces = lax.all_to_all(split_up(shard, dim, count), axis, 0, 0, tiled=True)
    return jnp.sum(pieces.astype(jnp.float32), axis=0)


def sum_in_two_steps(shard, axes, dim):
    far, near = axes
    pieces = split_up(shard, dim, lax.axis_size(far))
    nearer = summed_on_arrival(pieces, near, dim + 1)
    arrived = lax.all_to_all(
        nearer.astype(jnp.bfloat16), far, split_axis=0, concat_axis=0, tiled=True
    )
    return arrived.astype(jnp.float32).sum(axis=0)


def in_order(pieces, dim):
    lengths = list(pieces.shape[1:])
    lengths[dim] *= pieces.shape[0]
    return jnp.moveaxis(pieces, 0, dim).reshape(lengths)


def whole_of(shard, axes, dim):
    far, near = axes
    initial = sent_to_all(shard, far)
    pieces = jnp.swapaxes(sent_to_all(initial, near), 0, 1)
    return in_order(pieces.reshape(-1, *shard.shape), dim)


def run_blocks(
    query_h, key_h, value_h, gate_in, forget_logarithm, state_init, norm_init, peak_init
):
    span_len = BLOCK
    blocks_count = query_h.shape[0] // span_len
    query_b = query_h.reshape(blocks_count, span_len, query_h.shape[1])
    key_b = key_h.reshape(blocks_count, span_len, key_h.shape[1])
    value_b = value_h.reshape(blocks_count, span_len, value_h.shape[1])
    gate_b = gate_in.reshape(blocks_count, span_len)
    cum_local = jnp.cumsum(forget_logarithm.reshape(blocks_count, span_len), axis=1)
    cum_last = cum_local[:, -1]
    log_end = cum_last[:, None] - cum_local + gate_b

    def advance(carry, inputs):
        state_now, norm_now, peak_now = carry
        key_blk, value_blk, log_blk, last_blk = inputs
        peak_next = jnp.maximum(last_blk + peak_now, jnp.max(log_blk))
        decay_now = jnp.exp(last_blk + peak_now - peak_next)
        weights = jnp.exp(log_blk - peak_next)
        state_next = decay_now * state_now + jnp.einsum(
            "l,lv,lk->vk", weights, value_blk, key_blk, precision=lax.Precision.HIGHEST
        )
        norm_next = decay_now * norm_now + jnp.einsum(
            "l,lk->k", weights, key_blk, precision=lax.Precision.HIGHEST
        )
        return ((state_next, norm_next, peak_next), (state_now, norm_now, peak_now))

    carried, (state_prev, norm_prev, peak_prev) = lax.scan(
        advance, (state_init, norm_init, peak_init), (key_b, value_b, log_end, cum_last)
    )
    causal = jnp.tril(jnp.ones((span_len, span_len), dtype=bool))
    log_pair = cum_local[:, :, None] - cum_local[:, None, :] + gate_b[:, None, :]
    log_pair = jnp.where(causal[None], log_pair, -jnp.inf)
    inter_log = cum_local + peak_prev[:, None]
    peak_row = jnp.maximum(inter_log, jnp.max(log_pair, axis=2))
    scores = jnp.einsum("cjk,csk->cjs", query_b, key_b, precision=lax.Precision.HIGHEST) * jnp.exp(
        log_pair - peak_row[:, :, None]
    )
    inter_scale = jnp.exp(inter_log - peak_row)
    numer = jnp.einsum("cjs,csv->cjv", scores, value_b, precision=lax.Precision.HIGHEST)
    numer = numer + inter_scale[:, :, None] * jnp.einsum(
        "cjk,cvk->cjv", query_b, state_prev, precision=lax.Precision.HIGHEST
    )
    denominator = jnp.sum(scores, axis=2) + inter_scale * jnp.einsum(
        "cjk,ck->cj", query_b, norm_prev, precision=lax.Precision.HIGHEST
    )
    cell_out = numer / jnp.maximum(jnp.abs(denominator), jnp.exp(-peak_row))[:, :, None]
    return cell_out.reshape(query_h.shape[0], value_h.shape[1])


def by_heads(rows, heads_count):
    tok_count = rows.shape[0]
    return (
        rows.astype(jnp.float32)
        .reshape(tok_count, heads_count, rows.shape[1] // heads_count)
        .transpose(1, 0, 2)
    )


def rms_scaled(values_f32, gain):
    mean_square = jnp.mean(values_f32 * values_f32, axis=-1, keepdims=True)
    return values_f32 * lax.rsqrt(mean_square + 1e-06) * gain.astype(jnp.float32)


def joined(earlier, later):
    total_e, state_e, norm_e, peak_e = earlier
    total_l, state_l, norm_l, peak_l = later
    peak_both = jnp.maximum(total_l + peak_e, peak_l)
    weight_e = jnp.exp(total_l + peak_e - peak_both)
    weight_l = jnp.exp(peak_l - peak_both)
    state_both = weight_e[:, None, None] * state_e + weight_l[:, None, None] * state_l
    norm_both = weight_e[:, None] * norm_e + weight_l[:, None] * norm_l
    return (total_e + total_l, state_both, norm_both, peak_both)


def per_device(
    residual,
    queries,
    projected_key_rows,
    projected_value_rows,
    output_gate_logits,
    input_gate_logits,
    forget_gate_logits,
    extra_forget_logits,
    head_norm_gain,
    output_projection_weight,
    feedforward_norm_gain,
    feedforward_gate_weight,
    up_projection_weight,
    down_projection_weight,
):
    tok_here = queries.shape[0]
    heads_here = input_gate_logits.shape[0]
    own_rows = tok_here // lax.axis_size(TP)
    full_gate, full_up, full_down = sent_together(
        (feedforward_gate_weight, up_projection_weight, down_projection_weight), "sp", 0, 1
    )
    query_h = by_heads(queries, heads_here) * QK_DIM ** (-0.5)
    key_h = by_heads(projected_key_rows, heads_here)
    value_h = by_heads(projected_value_rows, heads_here)
    forget_logarithm = jax.nn.log_sigmoid(forget_gate_logits) + extra_forget_logits
    cum_shard = jnp.cumsum(forget_logarithm, axis=1)
    total_shard = cum_shard[:, -1]
    log_shard = total_shard[:, None] - cum_shard + input_gate_logits
    peak_shard = jnp.max(log_shard, axis=1)
    weight_shard = jnp.exp(log_shard - peak_shard[:, None])
    state_shard = jnp.einsum(
        "hl,hlv,hlk->hvk", weight_shard, value_h, key_h, precision=lax.Precision.HIGHEST
    )
    norm_shard = jnp.einsum("hl,hlk->hk", weight_shard, key_h, precision=lax.Precision.HIGHEST)
    identity = (
        jnp.zeros((heads_here,), jnp.float32),
        jnp.zeros_like(state_shard),
        jnp.zeros_like(norm_shard),
        jnp.full((heads_here,), -1e30, jnp.float32),
    )
    total_before, state_before, norm_before, peak_before = carried_in(
        (total_shard, state_shard, norm_shard, peak_shard), "sp", joined, identity
    )
    peak_in = jnp.maximum(peak_before, total_before)
    rescale = jnp.exp(peak_before - peak_in)
    state_in = rescale[:, None, None] * state_before
    norm_in = rescale[:, None] * norm_before
    cell_out = jax.vmap(run_blocks)(
        query_h, key_h, value_h, input_gate_logits, forget_logarithm, state_in, norm_in, peak_in
    )
    normed_heads = rms_scaled(cell_out, head_norm_gain.reshape(heads_here, 1, V_DIM))
    gated = (
        normed_heads.transpose(1, 0, 2).reshape(tok_here, heads_here * V_DIM)
        * jax.nn.sigmoid(output_gate_logits.astype(jnp.float32))
    ).astype(jnp.bfloat16)
    row_first = lax.axis_index(TP) * own_rows
    rows_part = gated
    attn_own = sum_in_two_steps(
        jnp.dot(rows_part, output_projection_weight, preferred_element_type=jnp.float32).astype(
            jnp.bfloat16
        ),
        ("tp_0", "tp_1"),
        0,
    )
    stream = (
        lax.dynamic_slice_in_dim(residual, row_first, own_rows, 0).astype(jnp.float32) + attn_own
    )
    normed_own = rms_scaled(stream, feedforward_norm_gain).astype(jnp.bfloat16)
    normed = whole_of(normed_own, ("tp_0", "tp_1"), 0)
    gate_pre = jnp.dot(normed, full_gate, preferred_element_type=jnp.float32)
    up_pre = jnp.dot(normed, full_up, preferred_element_type=jnp.float32)
    hidden = (jax.nn.silu(gate_pre) * up_pre).astype(jnp.bfloat16)
    rows_part = hidden
    ffn_own = lax.psum_scatter(
        lax.dot_general(
            rows_part, full_down, (((1,), (1,)), ((), ())), preferred_element_type=jnp.float32
        ).astype(jnp.bfloat16),
        TP,
        scatter_dimension=0,
        tiled=True,
    ).astype(jnp.float32)
    return (stream + 0.5 * ffn_own).astype(jnp.bfloat16)


def solution(mesh):
    split = Mesh(mesh.devices.reshape(mesh.shape["sp"], 4, 2), ("sp", "tp_0", "tp_1"))
    in_specs = (
        P("sp", None),
        P("sp", TP),
        P("sp", TP),
        P("sp", TP),
        P("sp", TP),
        P(TP, "sp"),
        P(TP, "sp"),
        P(TP, "sp"),
        P(TP),
        P(TP, None),
        P(),
        P("sp", TP),
        P("sp", TP),
        P("sp", TP),
    )
    out_specs = P(SP_TP, None)
    return jax.shard_map(
        per_device, mesh=split, in_specs=in_specs, out_specs=out_specs, check_vma=False
    )
```

profile of v0, /device:TPU:0, one launch (start us, length us, event | category | flops | bytes accessed | tf_op | source)
XLA Modules:
  0.0 308.6 jit_solution(9678271842075203368)
XLA Ops:
  6.6 3.2 %pad_maximum_fusion = bf16[256,4224]{1,0:T(8,128)(2,1)} fusion(bf16[256,1408]{1,0:T(8,128)(2,1)} %param.29, bf16[256,1408]{1,0:T(8,128)(2,1)} %param.28, bf16[256,1408]{1,0:T(8,128)(2,1)} %param.27), kind=kLoop, calls=%fused_computation.33 | loop fusion | flops 6488064 | bytes 4325376 | tf_op jit(solution)/shard_map/concatenate | solution.py:15
  12.8 1.3 broadcast_in_dim.84
  14.1 8.0 %all-to-all-start = ((f32[16,260,64]{1,2,0:T(8,128)}), f32[16,260,64]{1,2,0:T(8,128)}, u32[]{:S(2)}, u32[]{:S(2)}) async-start(f32[16,260,64]{1,2,0:T(8,128)} %broadcast_in_dim.84), calls=%async_computation | async-start | bytes 3145728 | tf_op jit(solution)/shard_map/all_to_all | solution.py:25
  26.7 33.8 %all-to-all-done = f32[16,260,64]{1,2,0:T(8,128)} async-done(((f32[16,260,64]{1,2,0:T(8,128)}), f32[16,260,64]{1,2,0:T(8,128)}, u32[]{:S(2)}, u32[]{:S(2)}) %all-to-all-start) | async-done | bytes 1064992 | tf_op jit(solution)/shard_map/all_to_all | solution.py:25
  60.5 1.6 fusion.58
  64.2 2.4 slice.194
  66.6 1.8 reshape_reshape.9
  70.3 27.1 %while.20 = (s32[]{:T(128)}, f32[2,128,64]{1,2,0:T(8,128)S(1)}, f32[2,64]{1,0:T(2,128)S(1)}, f32[2]{0:T(128)S(1)}, f32[8,2,128,64]{2,3,0,1:T(8,128)}, /*index=5*...) while((s32[]{:T(128)}, f32[2,128,64]{1,2,0:T(8,128)S(1)}, ...), condition=%wide.region_6.7_spmd, body=%wide.region_4.6_spmd.sunk | while | flops 12722694 | bytes 466693 | solution.py:131
  99.8 1.9 multiply_reduce_fusion.1
  102.0 2.2 convolution_convert_fusion
  104.8 8.1 %all_to_all.25 = bf16[2,4,64,4096]{3,2,1,0:T(8,128)(2,1)} all-to-all(bf16[2,4,64,4096]{3,2,1,0:T(8,128)(2,1)S(1)} %bitcast.165), channel_id=1, replica_groups=mesh['sp'=16,'tp_0'=4,'tp_1'=2] {'tp_1'}, dimensions={0} | all-to-all | bytes 8388608 | tf_op jit(solution)/shard_map/all_to_all | solution.py:77
  112.9 5.2 %reduce_sum.50 = bf16[4,64,4096]{2,1,0:T(8,128)(2,1)} reduce(bf16[2,4,64,4096]{3,2,1,0:T(8,128)(2,1)} %all_to_all.25, bf16[]{:T(256)} %constant.83.clone.1), dimensions={0}, to_apply=%region_10.11 | reduce | flops 1048576 | bytes 6291458 | tf_op jit(solution)/shard_map/reduce_sum | solution.py:78
  118.1 4.6 %all-to-all-start.2 = ((bf16[4,64,4096]{2,1,0:T(8,128)(2,1)}), bf16[4,64,4096]{2,1,0:T(8,128)(2,1)}, u32[]{:S(2)}, u32[]{:S(2)}) async-start(bf16[4,64,4096]{2,1,0:T(8,128)(2,1)} %reduce_sum.50), calls=%async_computation.2 | async-start | bytes 4194304 | tf_op jit(solution)/shard_map/all_to_all | solution.py:85
  122.8 26.9 %all-to-all-done.2 = bf16[4,64,4096]{2,1,0:T(8,128)(2,1)} async-done(((bf16[4,64,4096]{2,1,0:T(8,128)(2,1)}), bf16[4,64,4096]{2,1,0:T(8,128)(2,1)}, u32[]{:S(2)}, u32[]{:S(2)}) %all-to-all-start.2) | async-done | bytes 2097184 | tf_op jit(solution)/shard_map/all_to_all | solution.py:85
  149.7 2.1 convert_reduce_fusion
  151.8 1.7 multiply_reduce_fusion
  155.0 28.4 %all_to_all.26 = bf16[4,64,4096]{2,1,0:T(8,128)(2,1)S(1)} all-to-all(bf16[4,64,4096]{2,1,0:T(8,128)(2,1)S(1)} %broadcast_in_dim.139), channel_id=1, replica_groups=mesh['sp'=16,'tp_0'=4,'tp_1'=2] {'tp_0'}, dimensions={0} | all-to-all | bytes 4194304 | tf_op jit(solution)/shard_map/all_to_all | solution.py:25
  184.0 7.1 %all_to_all.27 = bf16[2,4,64,4096]{3,2,1,0:T(8,128)(2,1)S(1)} all-to-all(bf16[2,4,64,4096]{3,2,1,0:T(8,128)(2,1)S(1)} %broadcast_in_dim.140), channel_id=1, replica_groups=mesh['sp'=16,'tp_0'=4,'tp_1'=2] {'tp_1'}, dimensions={0} | all-to-all | bytes 8388608 | tf_op jit(solution)/shard_map/all_to_all | solution.py:25
  191.1 2.4 copy.168
  193.4 34.9 %all-gather.2.cloned.1.call-done = bf16[4096,4224]{1,0:T(8,128)(2,1)} async-done(((bf16[256,4224]{1,0:T(8,128)(2,1)}), bf16[4096,4224]{1,0:T(8,128)(2,1)}) %all-gather.2.cloned.1.call-update) | async-done | bytes 34603024 | tf_op jit(solution)/shard_map/all_gather | solution.py:16
  228.3 12.1 %fusion.12 = f32[512,1408]{1,0:T(8,128)} fusion(bf16[512,4096]{1,0:T(8,128)(2,1)} %bitcast.168, bf16[4096,4224]{1,0:T(8,128)(2,1)} %all-gather.2.cloned.1.call-done), kind=kOutput, calls=%fused_computation.21 | convolution fusion | flops 5905580032 | bytes 18612224 | tf_op jit(solution)/shard_map/dot_general | solution.py:249
  240.4 21.6 %fusion.14 = bf16[512,4096]{1,0:T(8,128)(2,1)} fusion(bf16[4096,4224]{1,0:T(8,128)(2,1)} %all-gather.2.cloned.1.call-done, bf16[512,4096]{1,0:T(8,128)(2,1)} %bitcast.169, f32[512,1408]{1,0:T(8,128)} %fusion.12), kind=kOutput, calls=%fused_computation.23 | convolution fusion | flops 11817582592 | bytes 34340864 | tf_op jit(solution)/shard_map/dot_general | solution.py:254
  262.0 37.6 %reduce-scatter.2.cloned.1.call-done = bf16[64,4096]{1,0:T(8,128)(2,1)} async-done(((bf16[512,4096]{1,0:T(8,128)(2,1)}), bf16[64,4096]{1,0:T(8,128)(2,1)}) %reduce-scatter.2.cloned.1.call-update) | async-done | bytes 524304 | tf_op jit(solution)/shard_map/reduce_scatter | solution.py:253
  299.6 2.2 add_convert_fusion
  (218 shorter events, 43.3 us)
Async XLA Ops:
  6.5 95.5 %copy-start = (bf16[256,4096]{1,0:T(8,128)(2,1)S(1)}, bf16[256,4096]{1,0:T(8,128)(2,1)}, u32[]{:S(2)}) copy-start(bf16[256,4096]{1,0:T(8,128)(2,1)} %param.25) | copy-start | bytes 6291460
  6.5 3.3 %copy-start.12 = (f32[2,512]{1,0:T(2,128)S(1)}, f32[2,512]{1,0:T(2,128)}, u32[]{:S(2)}) copy-start(f32[2,512]{1,0:T(2,128)} %param.23) | copy-start | bytes 12292
  6.5 3.3 %copy-start.13 = (f32[2,512]{1,0:T(2,128)S(1)}, f32[2,512]{1,0:T(2,128)}, u32[]{:S(2)}) copy-start(f32[2,512]{1,0:T(2,128)} %param.22) | copy-start | bytes 12292
  6.5 4.6 %copy-start.10 = (f32[2,512]{1,0:T(2,128)S(1)}, f32[2,512]{1,0:T(2,128)}, u32[]{:S(2)}) copy-start(f32[2,512]{1,0:T(2,128)} %param.21) | copy-start | bytes 12292
  6.5 5.0 %copy-start.8 = (bf16[512,128]{1,0:T(8,128)(2,1)S(1)}, bf16[512,128]{1,0:T(8,128)(2,1)}, u32[]{:S(2)}) copy-start(bf16[512,128]{1,0:T(8,128)(2,1)} %param.18) | copy-start | bytes 393220
  6.5 5.5 %copy-start.7 = (bf16[512,256]{1,0:T(8,128)(2,1)S(1)}, bf16[512,256]{1,0:T(8,128)(2,1)}, u32[]{:S(2)}) copy-start(bf16[512,256]{1,0:T(8,128)(2,1)} %param.19) | copy-start | bytes 786436
  6.6 221.7 %all-gather.2.cloned.1.call-start = ((), (), s32[]{:S(2)}) async-start(), calls=%async_computation.6 | async-start | bytes 36765696 | tf_op jit(solution)/shard_map/all_gather | solution.py:16
  9.8 13.6 %copy-start.9 = (bf16[512,128]{1,0:T(8,128)(2,1)S(1)}, bf16[512,128]{1,0:T(8,128)(2,1)}, u32[]{:S(2)}) copy-start(bf16[512,128]{1,0:T(8,128)(2,1)} %param.17) | copy-start | bytes 393220
  12.2 12.8 %copy-start.14 = (bf16[256]{0:T(256)(128)(2,1)S(1)}, bf16[256]{0:T(256)(128)(2,1)}, u32[]{:S(2)}) copy-start(bf16[256]{0:T(256)(128)(2,1)} %param.24) | copy-start | bytes 1540
  14.1 46.4 %all-to-all-start = ((f32[16,260,64]{1,2,0:T(8,128)}), f32[16,260,64]{1,2,0:T(8,128)}, u32[]{:S(2)}, u32[]{:S(2)}) async-start(f32[16,260,64]{1,2,0:T(8,128)} %broadcast_in_dim.84), calls=%async_computation | async-start | bytes 3145728 | tf_op jit(solution)/shard_map/all_to_all | solution.py:25
  22.5 4.2 %copy-start.5 = (bf16[2,8,64,64]{2,1,3,0:T(8,128)(2,1)}, bf16[2,8,64,64]{2,1,3,0:T(8,128)(2,1)S(1)}, u32[]{:S(2)}) copy-start(bf16[2,8,64,64]{2,1,3,0:T(8,128)(2,1)S(1)} %reshape.193) | copy-start | bytes 393220
  69.0 28.5 %copy-start.4 = (f32[2,512,64]{2,1,0:T(8,128)S(1)}, f32[2,512,64]{2,1,0:T(8,128)}, u32[]{:S(2)}) copy-start(f32[2,512,64]{2,1,0:T(8,128)} %copy.177) | copy-start | bytes 786436
  69.1 29.4 %copy-start.6 = (bf16[2,8,64,64]{2,1,3,0:T(8,128)(2,1)S(1)}, bf16[2,8,64,64]{2,1,3,0:T(8,128)(2,1)}, u32[]{:S(2)}) copy-start(bf16[2,8,64,64]{2,1,3,0:T(8,128)(2,1)} %copy-done.5) | copy-start | bytes 393220
  112.9 9.9 %copy-start.11 = (bf16[4096]{0:T(1024)(128)(2,1)S(1)}, bf16[4096]{0:T(1024)(128)(2,1)}, u32[]{:S(2)}) copy-start(bf16[4096]{0:T(1024)(128)(2,1)} %param.26) | copy-start | bytes 24580
  118.1 31.6 %all-to-all-start.2 = ((bf16[4,64,4096]{2,1,0:T(8,128)(2,1)}), bf16[4,64,4096]{2,1,0:T(8,128)(2,1)}, u32[]{:S(2)}, u32[]{:S(2)}) async-start(bf16[4,64,4096]{2,1,0:T(8,128)(2,1)} %reduce_sum.50), calls=%async_computation.2 | async-start | bytes 4194304 | tf_op jit(solution)/shard_map/all_to_all | solution.py:85
  122.8 176.8 %reduce-scatter.2.cloned.1.call-start = ((), (), s32[]{:S(2)}) async-start(), calls=%async_computation.7 | async-start | bytes 4718592 | tf_op jit(solution)/shard_map/reduce_scatter | solution.py:253
  151.8 31.6 %copy-start.2 = (f32[64,4096]{1,0:T(8,128)}, f32[64,4096]{1,0:T(8,128)S(1)}, u32[]{:S(2)}) copy-start(f32[64,4096]{1,0:T(8,128)S(1)} %convert_reduce_fusion) | copy-start | bytes 3145732
  240.4 61.4 %copy-start.1 = (bf16[256,4096]{1,0:T(8,128)(2,1)S(1)}, bf16[256,4096]{1,0:T(8,128)(2,1)}, u32[]{:S(2)}) copy-start(bf16[256,4096]{1,0:T(8,128)(2,1)} %param.25) | copy-start | bytes 6291460
  261.9 37.7 %copy-start.3 = (f32[64,4096]{1,0:T(8,128)S(1)}, f32[64,4096]{1,0:T(8,128)}, u32[]{:S(2)}) copy-start(f32[64,4096]{1,0:T(8,128)} %copy-done.2) | copy-start | bytes 3145732
Sparse Core Ops, SparseCore 0:
  9.9 218.3 all-gather.1
  262.1 37.4 reduce-scatter.1
where the time goes:
time: 310 us; the launch traced here: 309 us
  waiting for transfers between devices  133 us (43%)
  matrix products  50.5 us (16%)
  blocking collectives  43.7 us (14%)
  local copies, waits for them, and re-layouts  30.2 us (10%)
  other arithmetic  24.2 us (8%)
  between operations  13.9 us (4%)
  starting transfers between devices  12.7 us (4%)
    reduce_scatter x1, waiting for transfers between devices, per_device(): lax.psum_scatter(lax.dot_general(rows_part, full_down, (((1,), (1,)), (()...  37.6 us
    all_to_all x2, blocking collectives, sent_to_all(): lax.all_to_all(jnp.broadcast_to(shard[None], (count, *shard.shape)), axis...  35.5 us
    all_gather x1, waiting for transfers between devices, sent_together(): out, at, outs = (lax.all_gather(both, axis, axis=dim, tiled=True), 0, [])  34.9 us
    all_to_all x1, waiting for transfers between devices, sent_to_all(): lax.all_to_all(jnp.broadcast_to(shard[None], (count, *shard.shape)), axis...  33.8 us
    all_to_all x1, waiting for transfers between devices, sum_in_two_steps(): lax.all_to_all(nearer.astype(jnp.bfloat16), far, split_axis=0, concat_axi...  26.9 us
    dot_general x1, matrix products, per_device(): lax.dot_general(rows_part, full_down, (((1,), (1,)), ((), ())), preferred...  21.6 us
    dot_general x1, matrix products, per_device(): gate_pre = jnp.dot(normed, full_gate, preferred_element_type=jnp.float32)  12.1 us
    dynamic_slice x16, local copies, waits for them, and re-layouts, run_blocks(): lax.scan(advance, (state_init, norm_init, peak_init), (key_b, value_b, lo...  8.98 us
  transfers between devices with their start and end apart: 4, of which 4 were waited for; matrix products, arithmetic and copies ran while one was open for 21% of the time, Pallas kernels for 0%

commit v1 on v0

v1 whole, which is shorter than its diff:
```python
import functools

import jax
import jax.numpy as jnp
from jax import lax
from jax.experimental import pallas as pl
from jax.experimental.pallas import tpu as pltpu
from jax.sharding import PartitionSpec as P

MESH = pl.DeviceIdType.MESH
F32 = jnp.float32
BF16 = jnp.bfloat16
HI = lax.Precision.HIGHEST

TOK = 512
D = 4096
MAIN = 640
PADDED = 768
WIDE = 1408
ROWS = 64
CH = 512
SPLIT = {"gu": 176, "d": 128}
NSEM = 256


def nt(a, b, **kw):
    return lax.dot_general(a, b, (((1,), (1,)), ((), ())), preferred_element_type=F32, **kw)


def mm(a, b, **kw):
    return jnp.dot(a, b, preferred_element_type=F32, **kw)


def kernel(
    q_ref, k_ref, v_ref, og_ref, ig_ref, fl_ref, ef_ref, hg_ref, fgain_ref, wout_hbm, res_hbm, gate_hbm, up_hbm,
    down_hbm, out_ref,
    gu_w, d_w, gu_o, d_o, gu_b, d_b, tails, wout, res, nrm, pre, hid, part, a_d2d, a_r1, a_r2, stream, gated,
    f_d2d, f_sum, f_r1, f_r2, f_xr, x_state, x_rows, z_state, z_rows, num_s, row_s, l8,
    ssem, rsem, st_s, st_r, lsem,
):
    sp = lax.axis_index("sp")
    tp = lax.axis_index("tp")
    z, x = sp // 4, sp % 4
    y, c = tp // 2, tp % 2
    h = x % 2
    xp = x + 1 - 2 * h
    xq, xo = (x + 3 + 2 * h) % 4, (x + 2) % 4
    zl, zr, zo = (z + 3) % 4, (z + 1) % 4, (z + 2) % 4
    yl, yr, yo = (y + 3) % 4, (y + 1) % 4, (y + 2) % 4
    oc = 1 - c

    def at(zz, xx, yy, cc):
        return (zz * 4 + xx, yy * 2 + cc)

    core = at(z, x, y, oc)
    x_pair = at(z, xp, y, c)
    y_left, y_right = at(z, x, yl, c), at(z, x, yr, c)
    z_left, z_right = at(zl, x, y, c), at(zr, x, y, c)

    numbers = {}
    pending = {}

    def number(key):
        n = numbers.setdefault(key, len(numbers))
        assert n < NSEM
        return n

    def send(key, src, dst, dev):
        n = number(key)
        d = pltpu.make_async_remote_copy(
            src_ref=src, dst_ref=dst, send_sem=ssem.at[n], recv_sem=rsem.at[n], device_id=dev, device_id_type=MESH
        )
        d.start()
        pending[key] = d

    def arrived(key, ref):
        n = number(key)
        pltpu.make_async_remote_copy(
            src_ref=ref, dst_ref=ref, send_sem=ssem.at[n], recv_sem=rsem.at[n], device_id=core, device_id_type=MESH
        ).wait_recv()

    def sent(key):
        pending.pop(key).wait_send()

    def drain(*heads):
        for key in [k for k in pending if any(k[: len(h)] == h for h in heads)]:
            sent(key)

    barrier = pltpu.get_barrier_semaphore()
    x_others = {"p": at(z, xp, y, c), "q": at(z, xq, y, c), "o": at(z, xo, y, c)}
    z_others = [at(zz, x, y, c) for zz in (zl, zr, zo)]
    for dev in list(x_others.values()) + z_others + [y_left, y_right, core]:
        pl.semaphore_signal(barrier, inc=1, device_id=dev, device_id_type=MESH)

    def local(n, src, dst):
        return pltpu.make_async_copy(src, dst, lsem.at[n])

    own = sp
    oh = 1 - h
    keep = pl.ds(pl.multiple_of(h * MAIN, 128), MAIN)
    give = pl.ds(pl.multiple_of(oh * MAIN, 128), MAIN)
    last = pl.ds(2 * MAIN, 128)
    loads = [
        local(0, gate_hbm.at[:, last], tails.at[0]),
        local(1, up_hbm.at[:, last], tails.at[1]),
        local(2, gate_hbm.at[:, keep], gu_w.at[own, :, 0:MAIN]),
        local(3, up_hbm.at[:, keep], gu_w.at[own, :, PADDED:WIDE]),
        local(4, gate_hbm.at[:, give], gu_o.at[:, 0:MAIN]),
        local(5, up_hbm.at[:, give], gu_o.at[:, PADDED:WIDE]),
        local(6, down_hbm.at[:, keep], d_w.at[own, :, 0:MAIN]),
        local(7, down_hbm.at[:, last], d_w.at[own, :, MAIN:PADDED]),
        local(8, down_hbm.at[:, give], d_o.at[:, 0:MAIN]),
        local(9, down_hbm.at[:, last], d_o.at[:, MAIN:PADDED]),
    ]
    local_wout = local(10, wout_hbm, wout)
    local_res = local(11, res_hbm.at[pl.ds(tp * ROWS, ROWS)], res)
    for d in loads + [local_wout, local_res]:
        d.start()

    l8[...] = jnp.zeros_like(l8)
    fl = fl_ref[...]
    l8[0:2, :] = jnp.minimum(fl, 0.0) - jnp.log1p(jnp.exp(-jnp.abs(fl))) + ef_ref[...]
    logf = l8[...]
    i0 = lax.broadcasted_iota(jnp.int32, (TOK, TOK), 0)
    i1 = lax.broadcasted_iota(jnp.int32, (TOK, TOK), 1)
    cum_row = mm(logf, (i0 <= i1).astype(F32), precision=HI)
    cum_col = nt((i0 >= i1).astype(F32), logf, precision=HI)
    lane = lax.broadcasted_iota(jnp.int32, (1, 128), 1)
    row = lax.broadcasted_iota(jnp.int32, (128, 1), 0)
    a_row, total, w_row, peak = [], [], [], []
    for j in range(2):
        cr = cum_row[j : j + 1, :]
        a = ig_ref[j : j + 1, :] - cr
        t = cr[:, TOK - 1 : TOK]
        log_shard = t + a
        pk = jnp.max(log_shard, axis=1, keepdims=True)
        a_row.append(a)
        total.append(t)
        peak.append(pk)
        w_row.append(jnp.exp(log_shard - pk))
    k = k_ref[...]
    k_t = k.astype(F32).T
    k_tw = (k_t * jnp.where(row < 64, w_row[0], w_row[1])).astype(BF16)
    x_state[x] = jnp.where(row < 64, mm(k_tw, v_ref[:, 0:128]), mm(k_tw, v_ref[:, 128:256])).astype(BF16)
    norms = [mm(jnp.broadcast_to(w_row[j], (16, TOK)).astype(BF16), k)[0:1, :] for j in range(2)]
    x_rows[x, 0:1, :] = jnp.where(lane < 64, norms[0], norms[1])
    x_rows[x, 1:2, :] = jnp.where(lane < 64, total[0], total[1])
    x_rows[x, 2:3, :] = jnp.where(lane < 64, peak[0], peak[1])
    x_rows[x, 3:8, :] = jnp.zeros((5, 128), F32)

    loads[0].wait()
    loads[1].wait()
    gate_tail = tails[0].astype(F32)
    up_tail = pltpu.roll(tails[1].astype(F32), 64, 1)
    low = lane < 64
    mixed = [jnp.where(low, gate_tail, up_tail).astype(BF16), jnp.where(low, up_tail, gate_tail).astype(BF16)]
    gu_w[own, :, MAIN:PADDED] = jnp.where(h == 0, mixed[0], mixed[1])
    gu_o[:, MAIN:PADDED] = jnp.where(h == 0, mixed[1], mixed[0])
    for d in loads[2:]:
        d.wait()

    pl.semaphore_wait(barrier, 9)

    for name, dev in x_others.items():
        send(("xs", name), x_state.at[x], x_state.at[x], dev)
        send(("xt", name), x_rows.at[x], x_rows.at[x], dev)

    def joined(items):
        zero = jnp.zeros((1, 128), F32)
        total_all, tops = zero, []
        for there, _, total_e, peak_e, _ in reversed(items):
            tops.insert(0, jnp.where(there, total_all + peak_e, -1e30))
            total_all = total_all + jnp.where(there, total_e, 0.0)
        peak_all = functools.reduce(jnp.maximum, tops)
        norm, state = zero, jnp.zeros((128, 128), F32)
        for top, (there, norm_e, _, _, state_e) in zip(tops, items):
            w = jnp.exp(top - peak_all)
            norm = norm + jnp.where(there, w * norm_e, 0.0)
            wc = jnp.where(row < 64, w[:, 0:1], w[:, 64:65])
            state = state + jnp.where(there, wc * state_e.astype(F32), 0.0)
        return norm, total_all, peak_all, state

    def item(there, state_ref, rows_ref, e):
        return there, rows_ref[e, 0:1, :], rows_ref[e, 1:2, :], rows_ref[e, 2:3, :], state_ref[e]

    def z_state_copies(s):
        return [
            pltpu.make_async_remote_copy(
                src_ref=ref.at[3], dst_ref=ref.at[jnp.minimum(z, 2)], send_sem=st_s.at[n, s], recv_sem=st_r.at[n, jnp.minimum(z, 2)],
                device_id=at((z + s) % 4, x, y, c), device_id_type=MESH,
            )
            for n, ref in enumerate((z_state, z_rows))
        ]

    room = {"gu": gu_w, "d": d_w}
    other = {"gu": gu_o, "d": d_o}
    stage = {"gu": gu_b, "d": d_b}
    places = {"p": xp, "q": xq, "o": xo}
    turns = {"l": zl, "r": zr, "o": zo}
    sides = {"l": 0, "r": 1, "o": 2}

    def slot(mat, zz, xx, lo=0, hi=256):
        return room[mat].at[zz * 4 + xx, lo:hi]

    def x_own(mat, *names):
        for name in names:
            src = slot(mat, z, x) if name == "o" else other[mat]
            send(("x", mat, name), src, slot(mat, z, x), x_others[name])

    def cut(n):
        return (n // 2 + 15) // 16 * 16

    def z_own(mat):
        for side, dev in (("l", z_right), ("r", z_left)):
            send(("z", mat, "s", side), slot(mat, z, x), slot(mat, z, x), dev)

    def z_other(mat):
        for side, dev in (("l", z_right), ("r", z_left)):
            send(("zb", mat, side), other[mat].at[SPLIT[mat] : 256], stage[mat].at[sides[side]], dev)

    def z_own_forward(mat):
        arrived(("z", mat, "s", "l"), slot(mat, zl, x))
        send(("f", mat, "s", "l"), slot(mat, zl, x, 0, 128), slot(mat, zl, x, 0, 128), z_right)
        arrived(("z", mat, "s", "r"), slot(mat, zr, x))
        send(("f", mat, "s", "r"), slot(mat, zr, x, 128, 256), slot(mat, zr, x, 128, 256), z_left)

    def z_other_forward(mat):
        n = cut(256 - SPLIT[mat])
        arrived(("zb", mat, "l"), stage[mat].at[0])
        send(("fb", mat, "l"), stage[mat].at[0, 0:n], stage[mat].at[2, 0:n], z_right)
        arrived(("zb", mat, "r"), stage[mat].at[1])
        send(("fb", mat, "r"), stage[mat].at[1, n:], stage[mat].at[2, n:], z_left)

    def z_pass(mat, which):
        xx = places[which]
        arrived(("x", mat, which), slot(mat, z, xx))
        for side, dev in (("l", z_right), ("r", z_left)):
            send(("z", mat, which, side), slot(mat, z, xx, 0, SPLIT[mat]), slot(mat, z, xx, 0, SPLIT[mat]), dev)

    def z_pass_forward(mat, which):
        xx, end = places[which], SPLIT[mat]
        n = cut(end)
        arrived(("z", mat, which, "l"), slot(mat, zl, xx, 0, end))
        send(("f", mat, which, "l"), slot(mat, zl, xx, 0, n), slot(mat, zl, xx, 0, n), z_right)
        arrived(("z", mat, which, "r"), slot(mat, zr, xx, 0, end))
        send(("f", mat, which, "r"), slot(mat, zr, xx, n, end), slot(mat, zr, xx, n, end), z_left)

    def x_pass(mat, turn, *names):
        dst = slot(mat, turns[turn], x, SPLIT[mat], 256)
        for name in names:
            src = dst if name == "o" else stage[mat].at[sides[turn]]
            send(("xb", mat, turn, name), src, dst, x_others[name])

    def z_far_own(mat):
        arrived(("f", mat, "s", "l"), slot(mat, zo, x, 0, 128))
        arrived(("f", mat, "s", "r"), slot(mat, zo, x, 128, 256))

    def z_far_other(mat):
        n = cut(256 - SPLIT[mat])
        arrived(("fb", mat, "l"), stage[mat].at[2, 0:n])
        arrived(("fb", mat, "r"), stage[mat].at[2, n:])

    def x_done(mat, turn, *names):
        for which in names:
            arrived(("xb", mat, turn, which), slot(mat, turns[turn], places[which], SPLIT[mat], 256))

    def z_done(mat, *names):
        n = cut(SPLIT[mat])
        for which in names:
            arrived(("f", mat, which, "l"), slot(mat, zo, places[which], 0, n))
            arrived(("f", mat, which, "r"), slot(mat, zo, places[which], n, SPLIT[mat]))

    z_other("gu")
    x_own("gu", "p", "q", "o")
    for name, xx in places.items():
        arrived(("xs", name), x_state.at[xx])
        arrived(("xt", name), x_rows.at[xx])
    norm, total_all, peak_all, state = joined([item(True, x_state, x_rows, e) for e in range(4)])
    z_state[3] = state.astype(BF16)
    z_rows[3, 0:1, :] = norm
    z_rows[3, 1:2, :] = total_all
    z_rows[3, 2:3, :] = peak_all
    z_rows[3, 3:8, :] = jnp.zeros((5, 128), F32)
    for s in range(1, 4):
        @pl.when(z + s < 4)
        def _():
            for d in z_state_copies(s):
                d.start()
    z_own("gu")
    z_other("d")

    q8 = q_ref[...] * jnp.asarray(0.125, BF16)
    q_h = [jnp.where((lane < 64) == (j == 0), q8, jnp.zeros_like(q8)) for j in range(2)]
    for j in range(2):
        for r in range(4):
            n = (r + 1) * 128
            rows = slice(r * 128, n)
            s = nt(q_h[j][rows, :], k_ref[0:n, :])
            lp = cum_col[rows, j : j + 1] + a_row[j][:, 0:n]
            ti = lax.broadcasted_iota(jnp.int32, (128, n), 0) + r * 128
            si = lax.broadcasted_iota(jnp.int32, (128, n), 1)
            lp = jnp.where(si <= ti, lp, -jnp.inf)
            m = jnp.max(lp, axis=1, keepdims=True)
            p = s * jnp.exp(lp - m)
            row_s[j, rows, 0:1] = m
            row_s[j, rows, 1:2] = jnp.sum(p, axis=1, keepdims=True)
            num_s[j, rows, :] = mm(p.astype(BF16), v_ref[0:n, j * 128 : (j + 1) * 128])

    for e in range(3):
        @pl.when(e < z)
        def _():
            for n, ref in enumerate((z_state, z_rows)):
                pltpu.make_async_remote_copy(
                    src_ref=ref.at[e], dst_ref=ref.at[e], send_sem=st_s.at[n, 0], recv_sem=st_r.at[n, e],
                    device_id=core, device_id_type=MESH,
                ).wait_recv()

    norm, total_all, peak_all, state = joined(
        [item(e < z, z_state, z_rows, e) for e in range(3)] + [item(e < x, x_state, x_rows, e) for e in range(3)]
    )
    peak_in = jnp.maximum(peak_all, total_all)
    rescale = jnp.exp(peak_all - peak_in)
    norm = norm * rescale
    state = (state * jnp.where(row < 64, rescale[:, 0:1], rescale[:, 64:65])).astype(BF16)
    for j in range(2):
        il = cum_col[:, j : j + 1] + peak_in[:, 64 * j : 64 * j + 1]
        m = row_s[j, :, 0:1]
        pr = jnp.maximum(il, m)
        e1, e2 = jnp.exp(m - pr), jnp.exp(il - pr)
        numer = e1 * num_s[j] + e2 * mm(q_h[j], state)
        denom = e1 * row_s[j, :, 1:2] + e2 * jnp.sum(q_h[j].astype(F32) * norm, axis=1, keepdims=True)
        cell = numer / jnp.maximum(jnp.abs(denom), jnp.exp(-pr))
        mean = jnp.mean(cell * cell, axis=1, keepdims=True)
        cols = slice(j * 128, (j + 1) * 128)
        g = cell * lax.rsqrt(mean + 1e-06) * hg_ref[cols].astype(F32)[None, :] * jax.nn.sigmoid(og_ref[:, cols].astype(F32))
        gated[:, cols] = g.astype(BF16)

    local_wout.wait()
    local_res.wait()
    def cols_of(i):
        return slice(i * CH, (i + 1) * CH)

    for i in range(4):
        for n in range(2):
            r = mm(gated[...], wout[:, cols_of(2 * i + n)]).astype(BF16)
            part[i, :, n] = r.reshape(4, 2, ROWS, CH)
        send(("ad", i), part.at[i, :, :, oc], a_d2d.at[i], core)
    for i in range(4):
        arrived(("ad", i), a_d2d.at[i])
        f_sum[4 + i] = (part[i, :, :, c].astype(F32) + a_d2d[i].astype(F32)).astype(BF16)
        send(("a1l", i), f_sum.at[4 + i, yo, :, 0:32], a_r1.at[i, 0], y_right)
        send(("a1r", i), f_sum.at[4 + i, yo, :, 32:64], a_r1.at[i, 1], y_left)
    z_pass("gu", "p")
    for i in range(4):
        arrived(("a1l", i), a_r1.at[i, 0])
        f_sum[4 + i, yr, :, 0:32] = (f_sum[4 + i, yr, :, 0:32].astype(F32) + a_r1[i, 0].astype(F32)).astype(BF16)
        send(("a2l", i), f_sum.at[4 + i, yr], a_r2.at[i, 0], y_right)
        arrived(("a1r", i), a_r1.at[i, 1])
        f_sum[4 + i, yl, :, 32:64] = (f_sum[4 + i, yl, :, 32:64].astype(F32) + a_r1[i, 1].astype(F32)).astype(BF16)
        send(("a2r", i), f_sum.at[4 + i, yl], a_r2.at[i, 1], y_left)
    z_own_forward("gu")
    z_pass("gu", "q")
    square = jnp.zeros((ROWS, 1), F32)
    for i in range(4):
        arrived(("a2l", i), a_r2.at[i, 0])
        arrived(("a2r", i), a_r2.at[i, 1])
        for n in range(2):
            cols = cols_of(2 * i + n)
            s = part[i, y, n, c].astype(F32) + a_d2d[i, y, n].astype(F32)
            s = s + a_r2[i, 0, n].astype(F32) + a_r2[i, 1, n].astype(F32) + res[:, cols].astype(F32)
            stream[:, cols] = s
            square = square + jnp.sum(s * s, axis=1, keepdims=True)
    scale = lax.rsqrt(square * (1.0 / D) + 1e-06)
    for i in range(8):
        cols = cols_of(i)
        nrm[y, h, c, :, cols] = (stream[:, cols] * scale * fgain_ref[cols].astype(F32)[None, :]).astype(BF16)

    def rows_of(yy, pp, cc, half=None):
        ref = nrm.at[yy, pp, cc]
        return ref if half is None else ref.at[half * 32 : (half + 1) * 32]

    def pass_on(key, yy, pp, dev, half=None):
        send(key, rows_of(yy, pp, c, half), rows_of(yy, pp, c, half), dev)

    pass_on(("ny", 0, "l"), y, h, y_right)
    pass_on(("ny", 0, "r"), y, h, y_left)
    pass_on(("nx",), y, h, x_pair)
    pass_on(("nc", 0, 0), y, h, core)
    z_other_forward("gu")
    for turn in ("l", "r"):
        x_pass("gu", turn, "p", "q", "o")
    x_own("d", "p", "q")
    z_pass("gu", "o")
    for s in range(1, 4):
        @pl.when(z + s < 4)
        def _():
            for d in z_state_copies(s):
                d.wait_send()
    drain(("xs",), ("xt",), ("ad",), ("a1l",), ("a1r",), ("a2l",), ("a2r",), ("zb", "gu"), ("z", "gu", "s"), ("x", "gu"))
    arrived(("nx",), rows_of(y, oh, c))
    pass_on(("ny", 1, "l"), y, oh, y_right)
    pass_on(("ny", 1, "r"), y, oh, y_left)
    pass_on(("nc", 0, 1), y, oh, core)

    def ring_forward(n, pp):
        arrived(("ny", n, "l"), rows_of(yl, pp, c))
        pass_on(("nf", n, "l"), yl, pp, y_right, 0)
        pass_on(("nc", 1, n), yl, pp, core)
        arrived(("ny", n, "r"), rows_of(yr, pp, c))
        pass_on(("nf", n, "r"), yr, pp, y_left, 1)
        pass_on(("nc", 2, n), yr, pp, core)

    def ring_last(n, pp):
        arrived(("nf", n, "l"), rows_of(yo, pp, c, 0))
        arrived(("nf", n, "r"), rows_of(yo, pp, c, 1))
        pass_on(("nc", 3, n), yo, pp, core)

    def from_core(place, yy):
        arrived(("nc", place, 0), rows_of(yy, h, oc))
        arrived(("nc", place, 1), rows_of(yy, oh, oc))

    def gu_tile(yy, kz, first):
        xs = nrm[yy, :, :, :, pl.ds(pl.multiple_of(kz * 1024, 1024), 1024)].reshape(256, 1024)
        for lo, hi in ((0, 512), (512, 1024), (1024, 1408)):
            r = mm(xs, gu_w[pl.ds(kz * 4, 4), :, lo:hi].reshape(1024, hi - lo))
            pre[yy, :, lo:hi] = r if first else pre[yy, :, lo:hi] + r

    def nth(base, i):
        return (base + i + i // 2 - 2 * (i // 3)) % 4

    ring_forward(0, h)
    z_pass_forward("gu", "p")
    from_core(0, y)
    gu_tile(y, z, True)
    drain(("zb",), ("nx",), ("ny", 0), ("nc", 0), ("z", "gu", "p"), ("f", "gu", "s"))
    z_pass_forward("gu", "q")
    z_far_own("gu")
    z_far_other("gu")
    x_pass("gu", "o", "p", "q", "o")
    x_own("d", "o")
    z_other_forward("d")
    for turn in ("l", "r"):
        x_pass("d", turn, "p", "q")
    ring_forward(1, oh)
    from_core(1, yl)
    from_core(2, yr)

    @pl.loop(0, 2)
    def _(i):
        gu_tile((y + 1 + 2 * i) % 4, z, True)

    ring_last(0, h)
    z_pass_forward("gu", "o")
    z_own("d")
    z_pass("d", "p")
    z_pass("d", "q")
    x_done("gu", "l", "p", "q", "o")

    @pl.loop(0, 3)
    def _(i):
        gu_tile((y + i + i // 2) % 4, zl, False)

    ring_last(1, oh)
    x_done("gu", "r", "p", "q", "o")

    @pl.loop(0, 3)
    def _(i):
        gu_tile((y + i + i // 2) % 4, zr, False)

    from_core(3, yo)
    gu_tile(yo, z, True)

    @pl.loop(0, 2)
    def _(i):
        gu_tile(yo, (z + 1 + 2 * i) % 4, False)

    drain(("ny",), ("nf",), ("nc",), ("z", "gu"), ("fb",), ("x", "d", "p"), ("x", "d", "q"), ("xb", "gu"))
    drain(("f", "gu", "p"), ("f", "gu", "q"))
    z_done("gu", "p", "q")
    x_done("gu", "o", "p", "q", "o")

    def gu_slot(yy, zz, xx):
        k = zz * 4 + xx
        xs = nrm[yy, :, :, :, pl.ds(pl.multiple_of(k * 256, 256), 256)].reshape(256, 256)
        for lo, hi in ((0, 512), (512, 1024), (1024, 1408)):
            pre[yy, :, lo:hi] += mm(xs, gu_w[k, :, lo:hi])

    @pl.loop(0, 4)
    def _(yy):
        for xx in (x, xp, xq):
            gu_slot(yy, zo, xx)

    z_done("gu", "o")

    @pl.loop(0, 4)
    def _(yy):
        gu_slot(yy, zo, xo)
        rows = pl.ds(pl.multiple_of(yy * 256, 256), 256)
        hid[rows, 0:MAIN] = (jax.nn.silu(pre[yy, :, 0:MAIN]) * pre[yy, :, PADDED:WIDE]).astype(BF16)
        tail = pre[yy, :, MAIN:PADDED]
        both = jax.nn.silu(tail) * pltpu.roll(tail, 64, 1)
        hid[rows, MAIN:PADDED] = jnp.where(low == (h == 0), both, 0.0).astype(BF16)

    near, away = x // 2, 1 - x // 2
    order = [(z, near), (z, away), (zl, near), (zr, near), (zl, away), (zr, away), (zo, near), (zo, away)]

    def down(i):
        zz, j = order[i]
        if i >= 4:
            sent(("fd", i - 4))

        @pl.loop(0, 2)
        def _(s):
            r = nt(hid[...], d_w[zz * 4 + j * 2 + s]).astype(BF16)
            part[i % 4, :, :, :, :, pl.ds(pl.multiple_of(s * 256, 256), 256)] = r.reshape(4, 2, 2, ROWS, 256)

        send(("fd", i), part.at[i % 4, :, :, oc], f_d2d.at[i], core)

    def sum_cores(i):
        arrived(("fd", i), f_d2d.at[i])
        f_sum[i] = (part[i % 4, :, :, c].astype(F32) + f_d2d[i].astype(F32)).astype(BF16)
        send(("f1l", i), f_sum.at[i, yo, :, 0:32], f_r1.at[i, 0], y_right)
        send(("f1r", i), f_sum.at[i, yo, :, 32:64], f_r1.at[i, 1], y_left)

    def sum_far(i):
        arrived(("f1l", i), f_r1.at[i, 0])
        f_sum[i, yr, :, 0:32] = (f_sum[i, yr, :, 0:32].astype(F32) + f_r1[i, 0].astype(F32)).astype(BF16)
        send(("f2l", i), f_sum.at[i, yr], f_r2.at[i, 0], y_right)
        arrived(("f1r", i), f_r1.at[i, 1])
        f_sum[i, yl, :, 32:64] = (f_sum[i, yl, :, 32:64].astype(F32) + f_r1[i, 1].astype(F32)).astype(BF16)
        send(("f2r", i), f_sum.at[i, yl], f_r2.at[i, 1], y_left)

    def ring_sum(i, pp):
        return f_sum[i, y, pp].astype(F32) + f_r2[i, 0, pp].astype(F32) + f_r2[i, 1, pp].astype(F32)

    def sum_near(i):
        if i >= 2:
            drain(("f1l", i - 1), ("f1r", i - 1), ("f2l", i - 2), ("f2r", i - 2), ("fx", i - 2))
        arrived(("f2l", i), f_r2.at[i, 0])
        arrived(("f2r", i), f_r2.at[i, 1])
        f_sum[i, y, oh] = ring_sum(i, oh).astype(BF16)
        send(("fx", i), f_sum.at[i, y, oh], f_xr.at[i], x_pair)

    def finish(i):
        zz, j = order[i]
        arrived(("fx", i), f_xr.at[i])
        cols = pl.ds(pl.multiple_of(zz * 1024 + j * CH, CH), CH)
        out_ref[:, cols] = (stream[:, cols] + 0.5 * (ring_sum(i, h) + f_xr[i].astype(F32))).astype(BF16)

    down(0)
    z_pass("d", "o")
    down(1)
    sum_cores(0)
    z_own_forward("d")
    for turn in ("l", "r"):
        x_pass("d", turn, "o")
    z_far_other("d")
    x_pass("d", "o", "p", "q")
    sum_cores(1)
    sum_far(0)
    z_pass_forward("d", "p")
    x_done("d", "l", "p")
    down(2)
    x_done("d", "r", "p")
    down(3)
    sum_far(1)
    sum_cores(2)
    sum_near(0)
    sum_cores(3)
    z_pass_forward("d", "q")
    sum_near(1)
    sum_far(2)
    z_pass_forward("d", "o")
    x_done("d", "l", "q", "o")
    down(4)
    x_done("d", "r", "q", "o")
    down(5)
    sum_far(3)
    z_far_own("d")
    x_pass("d", "o", "o")
    sum_cores(4)
    sum_cores(5)
    sum_near(2)
    drain(("x", "d"), ("z", "d"), ("f", "gu"), ("xb", "d", "l"), ("xb", "d", "r"), ("f", "d", "s"))
    z_done("d", "p")
    x_done("d", "o", "p")
    down(6)
    sum_far(4)
    sum_near(3)
    sum_cores(6)
    z_done("d", "q", "o")
    x_done("d", "o", "q", "o")
    down(7)
    sum_far(5)
    sum_near(4)
    sum_cores(7)
    finish(0)
    sum_far(6)
    finish(1)
    sum_near(5)
    finish(2)
    sum_far(7)
    for i in range(3, 6):
        finish(i)
    sum_near(6)
    sum_near(7)
    finish(6)
    drain(("f",), ("xb",), ("fd",))
    finish(7)

    for key in list(pending):
        sent(key)


def per_device(
    residual, queries, keys, values, output_gate, input_gate, forget_gate, extra_forget, head_gain, wout, ffn_gain,
    gate_w, up_w, down_w,
):
    vmem = pl.BlockSpec(memory_space=pltpu.VMEM)
    anywhere = pl.BlockSpec(memory_space=pl.ANY)
    scratch = [
        pltpu.VMEM((16, 256, WIDE), BF16),
        pltpu.VMEM((16, 256, PADDED), BF16),
        pltpu.VMEM((256, WIDE), BF16),
        pltpu.VMEM((256, PADDED), BF16),
        pltpu.VMEM((3, 256 - SPLIT["gu"], WIDE), BF16),
        pltpu.VMEM((3, 256 - SPLIT["d"], PADDED), BF16),
        pltpu.VMEM((2, 256, 128), BF16),
        pltpu.VMEM((256, D), BF16),
        pltpu.VMEM((ROWS, D), BF16),
        pltpu.VMEM((4, 2, 2, ROWS, D), BF16),
        pltpu.VMEM((4, 256, WIDE), F32),
        pltpu.VMEM((1024, PADDED), BF16),
        pltpu.VMEM((4, 4, 2, 2, ROWS, CH), BF16),
        pltpu.VMEM((4, 4, 2, ROWS, CH), BF16),
        pltpu.VMEM((4, 2, 2, 32, CH), BF16),
        pltpu.VMEM((4, 2, 2, ROWS, CH), BF16),
        pltpu.VMEM((ROWS, D), F32),
        pltpu.VMEM((TOK, 256), BF16),
        pltpu.VMEM((8, 4, 2, ROWS, CH), BF16),
        pltpu.VMEM((8, 4, 2, ROWS, CH), BF16),
        pltpu.VMEM((8, 2, 2, 32, CH), BF16),
        pltpu.VMEM((8, 2, 2, ROWS, CH), BF16),
        pltpu.VMEM((8, ROWS, CH), BF16),
        pltpu.VMEM((4, 128, 128), BF16),
        pltpu.VMEM((4, 8, 128), F32),
        pltpu.VMEM((4, 128, 128), BF16),
        pltpu.VMEM((4, 8, 128), F32),
        pltpu.VMEM((2, TOK, 128), F32),
        pltpu.VMEM((2, TOK, 2), F32),
        pltpu.VMEM((8, TOK), F32),
        pltpu.SemaphoreType.DMA((NSEM,)),
        pltpu.SemaphoreType.DMA((NSEM,)),
        pltpu.SemaphoreType.DMA((2, 4)),
        pltpu.SemaphoreType.DMA((2, 4)),
        pltpu.SemaphoreType.DMA((12,)),
    ]
    return pl.pallas_call(
        kernel,
        out_shape=jax.ShapeDtypeStruct((ROWS, D), BF16),
        in_specs=[vmem] * 9 + [anywhere] * 5,
        out_specs=vmem,
        scratch_shapes=scratch,
        compiler_params=pltpu.CompilerParams(
            collective_id=0, has_side_effects=True, vmem_limit_bytes=67_043_328
        ),
        name="layer",
    )(
        queries, keys, values, output_gate, input_gate, forget_gate, extra_forget,
        head_gain, ffn_gain, wout, residual, gate_w, up_w, down_w,
    )


def solution(mesh):
    tp_sp = P("tp", "sp")
    rows = P("sp", "tp")
    in_specs = (
        P("sp", None), rows, rows, rows, rows, tp_sp, tp_sp, tp_sp, P("tp"), P("tp", None), P(), rows, rows, rows,
    )
    return jax.shard_map(
        per_device, mesh=mesh, in_specs=in_specs, out_specs=P(("sp", "tp"), None), check_vma=False
    )
```

time: 310 us -> 155 us (0.50)
  Pallas kernels: 0 us -> 153 us
  waiting for transfers between devices: 133 us -> 0 us
  matrix products: 50.5 us -> 0 us
  blocking collectives: 43.7 us -> 0 us
  local copies, waits for them, and re-layouts: 30.2 us -> 1.87 us
  other arithmetic: 24.2 us -> 0 us
  between operations: 13.9 us -> 0.01 us
  starting transfers between devices: 12.7 us -> 0 us
    pallas_call x0 -> x1, Pallas kernels: none -> 153 us  [per_device(): pl.pallas_call(kernel, out_shape=jax.ShapeDtypeStruct((ROWS, D), BF16), i...]
    all_to_all x2 -> x0, waiting for transfers between devices: 60.7 us -> none  [the longest x1 33.8 us: sent_to_all(): lax.all_to_all(jnp.broadcast_to(shard[None], (count, *shard.shape)), axis...]
    dot_general x25 -> x0, matrix products: 50.5 us -> none  [the longest x1 21.6 us: per_device(): lax.dot_general(rows_part, full_down, (((1,), (1,)), ((), ())), preferred...]
    all_to_all x3 -> x0, blocking collectives: 43.7 us -> none  [the longest x2 35.5 us: sent_to_all(): lax.all_to_all(jnp.broadcast_to(shard[None], (count, *shard.shape)), axis...]
    reduce_scatter x1 -> x0, waiting for transfers between devices: 37.6 us -> none  [per_device(): lax.psum_scatter(lax.dot_general(rows_part, full_down, (((1,), (1,)), (()...]
    all_gather x1 -> x0, waiting for transfers between devices: 34.9 us -> none  [sent_together(): out, at, outs = (lax.all_gather(both, axis, axis=dim, tiled=True), 0, [])]
    all_to_all x2 -> x0, starting transfers between devices: 12.7 us -> none  [the longest x1 8.03 us: sent_to_all(): lax.all_to_all(jnp.broadcast_to(shard[None], (count, *shard.shape)), axis...]
    reduce_sum x3 -> x0, other arithmetic: 9 us -> none  [the longest x1 5.23 us: summed_on_arrival(): return jnp.sum(pieces.astype(jnp.float32), axis=0)]
  transfers between devices with their start and end apart: 4 -> 0, of which waited for: 4 -> 0; matrix products, arithmetic and copies ran while one was open for 21% -> 0% of each run, Pallas kernels for 0% -> 0%
where the time goes in v1:
time: 155 us
  Pallas kernels  153 us (99%)
  local copies, waits for them, and re-layouts  1.87 us (1%)
    pallas_call x1, Pallas kernels, per_device(): pl.pallas_call(kernel, out_shape=jax.ShapeDtypeStruct((ROWS, D), BF16), i...  153 us

profile of v1, /device:TPU:0, one launch (start us, length us, event | category | flops | bytes accessed | tf_op | source)
XLA Modules:
  0.0 154.7 jit_solution(18109272717762279895)
XLA Ops:
  0.0 152.8 %layer.1 = bf16[64,4096]{1,0:T(8,128)(2,1)} custom-call(bf16[512,128]{1,0:T(8,128)(2,1)} %q_ref.1, bf16[512,128]{1,0:T(8,128)(2,1)} %k_ref.1, bf16[512,256]{1,0:T(8,128)(2,1)} %v_ref.1, bf16[512,256]{1,0:T(8,128)(2,1)} %og_ref.1, f32[2,512]{1,0:T(2,128)} %ig_ref.1, f32[2,512]{1,0:T(2,128)} %fl_ref.1, f32[2,512]{1,0:T(2,128)} %ef_ref.1, ...), custom_call_target="tpu_custom_call" | custom-call | tf_op jit(solution)/shard_map/layer/pallas_call | solution.py:658
  152.8 1.9 %copy.16 = bf16[64,4096]{1,0:T(8,128)(2,1)} copy(bf16[64,4096]{1,0:T(8,128)(2,1)} %layer.1) | data formatting | bytes 1048576

commit v2 on v1

--- a/solution.py
+++ b/solution.py
@@ -20,7 +20,8 @@
 ROWS = 64
 CH = 512
 SPLIT = {"gu": 176, "d": 128}
-NSEM = 256
+NSEM = 143
+NSEND = 58
 
 
 def nt(a, b, **kw):
@@ -32,8 +33,9 @@
 
 
 def kernel(
-    q_ref, k_ref, v_ref, og_ref, ig_ref, fl_ref, ef_ref, hg_ref, fgain_ref, wout_hbm, res_hbm, gate_hbm, up_hbm,
+    q_hbm, k_hbm, v_hbm, og_hbm, ig_hbm, fl_hbm, ef_hbm, hg_hbm, fgain_hbm, wout_hbm, res_hbm, gate_hbm, up_hbm,
     down_hbm, out_ref,
+    q_ref, k_ref, v_ref, og_ref, ig_ref, fl_ref, ef_ref, hg_ref, fgain_ref,
     gu_w, d_w, gu_o, d_o, gu_b, d_b, tails, wout, res, nrm, pre, hid, part, a_d2d, a_r1, a_r2, stream, gated,
     f_d2d, f_sum, f_r1, f_r2, f_xr, x_state, x_rows, z_state, z_rows, num_s, row_s, l8,
     ssem, rsem, st_s, st_r, lsem,
@@ -59,28 +61,32 @@
 
     numbers = {}
     pending = {}
+    free = list(range(NSEND))
 
     def number(key):
         n = numbers.setdefault(key, len(numbers))
         assert n < NSEM
         return n
 
-    def send(key, src, dst, dev):
-        n = number(key)
+    def send(key, src, dst, dev, at_key=None):
+        slot_s = free.pop(0)
         d = pltpu.make_async_remote_copy(
-            src_ref=src, dst_ref=dst, send_sem=ssem.at[n], recv_sem=rsem.at[n], device_id=dev, device_id_type=MESH
+            src_ref=src, dst_ref=dst, send_sem=ssem.at[slot_s], recv_sem=rsem.at[number(at_key or key)], device_id=dev,
+            device_id_type=MESH,
         )
         d.start()
-        pending[key] = d
+        pending[key] = d, slot_s
 
     def arrived(key, ref):
         n = number(key)
         pltpu.make_async_remote_copy(
-            src_ref=ref, dst_ref=ref, send_sem=ssem.at[n], recv_sem=rsem.at[n], device_id=core, device_id_type=MESH
+            src_ref=ref, dst_ref=ref, send_sem=ssem.at[0], recv_sem=rsem.at[n], device_id=core, device_id_type=MESH
         ).wait_recv()
 
     def sent(key):
-        pending.pop(key).wait_send()
+        d, slot_s = pending.pop(key)
+        d.wait_send()
+        free.append(slot_s)
 
     def drain(*heads):
         for key in [k for k in pending if any(k[: len(h)] == h for h in heads)]:
@@ -114,8 +120,19 @@
     ]
     local_wout = local(10, wout_hbm, wout)
     local_res = local(11, res_hbm.at[pl.ds(tp * ROWS, ROWS)], res)
-    for d in loads + [local_wout, local_res]:
+    first = [
+        local(12 + n, src, dst)
+        for n, (src, dst) in enumerate(
+            (
+                (fl_hbm, fl_ref), (ef_hbm, ef_ref), (ig_hbm, ig_ref), (k_hbm, k_ref), (v_hbm, v_ref), (q_hbm, q_ref),
+                (og_hbm, og_ref), (hg_hbm, hg_ref), (fgain_hbm, fgain_ref),
+            )
+        )
+    ]
+    for d in first + loads + [local_wout, local_res]:
         d.start()
+    for d in first[:5]:
+        d.wait()
 
     l8[...] = jnp.zeros_like(l8)
     fl = fl_ref[...]
@@ -140,8 +157,11 @@
         w_row.append(jnp.exp(log_shard - pk))
     k = k_ref[...]
     k_t = k.astype(F32).T
-    k_tw = (k_t * jnp.where(row < 64, w_row[0], w_row[1])).astype(BF16)
-    x_state[x] = jnp.where(row < 64, mm(k_tw, v_ref[:, 0:128]), mm(k_tw, v_ref[:, 128:256])).astype(BF16)
+    k_tw = k_t * jnp.where(row < 64, w_row[0], w_row[1])
+    k_hi = k_tw.astype(BF16)
+    k_lo = (k_tw - k_hi.astype(F32)).astype(BF16)
+    states = [mm(k_hi, v_ref[:, n : n + 128]) + mm(k_lo, v_ref[:, n : n + 128]) for n in (0, 128)]
+    x_state[x] = jnp.where(row < 64, states[0], states[1])
     norms = [mm(jnp.broadcast_to(w_row[j], (16, TOK)).astype(BF16), k)[0:1, :] for j in range(2)]
     x_rows[x, 0:1, :] = jnp.where(lane < 64, norms[0], norms[1])
     x_rows[x, 1:2, :] = jnp.where(lane < 64, total[0], total[1])
@@ -177,7 +197,7 @@
             w = jnp.exp(top - peak_all)
             norm = norm + jnp.where(there, w * norm_e, 0.0)
             wc = jnp.where(row < 64, w[:, 0:1], w[:, 64:65])
-            state = state + jnp.where(there, wc * state_e.astype(F32), 0.0)
+            state = state + jnp.where(there, wc * state_e, 0.0)
         return norm, total_all, peak_all, state
 
     def item(there, state_ref, rows_ref, e):
@@ -276,7 +296,7 @@
         arrived(("xs", name), x_state.at[xx])
         arrived(("xt", name), x_rows.at[xx])
     norm, total_all, peak_all, state = joined([item(True, x_state, x_rows, e) for e in range(4)])
-    z_state[3] = state.astype(BF16)
+    z_state[3] = state
     z_rows[3, 0:1, :] = norm
     z_rows[3, 1:2, :] = total_all
     z_rows[3, 2:3, :] = peak_all
@@ -287,8 +307,9 @@
             for d in z_state_copies(s):
                 d.start()
     z_own("gu")
-    z_other("d")
-
+
+    for d in first[5:]:
+        d.wait()
     q8 = q_ref[...] * jnp.asarray(0.125, BF16)
     q_h = [jnp.where((lane < 64) == (j == 0), q8, jnp.zeros_like(q8)) for j in range(2)]
     for j in range(2):
@@ -321,13 +342,15 @@
     peak_in = jnp.maximum(peak_all, total_all)
     rescale = jnp.exp(peak_all - peak_in)
     norm = norm * rescale
-    state = (state * jnp.where(row < 64, rescale[:, 0:1], rescale[:, 64:65])).astype(BF16)
+    state = state * jnp.where(row < 64, rescale[:, 0:1], rescale[:, 64:65])
+    s_hi = state.astype(BF16)
+    s_lo = (state - s_hi.astype(F32)).astype(BF16)
     for j in range(2):
         il = cum_col[:, j : j + 1] + peak_in[:, 64 * j : 64 * j + 1]
         m = row_s[j, :, 0:1]
         pr = jnp.maximum(il, m)
         e1, e2 = jnp.exp(m - pr), jnp.exp(il - pr)
-        numer = e1 * num_s[j] + e2 * mm(q_h[j], state)
+        numer = e1 * num_s[j] + e2 * (mm(q_h[j], s_hi) + mm(q_h[j], s_lo))
         denom = e1 * row_s[j, :, 1:2] + e2 * jnp.sum(q_h[j].astype(F32) * norm, axis=1, keepdims=True)
         cell = numer / jnp.maximum(jnp.abs(denom), jnp.exp(-pr))
         mean = jnp.mean(cell * cell, axis=1, keepdims=True)
@@ -354,16 +377,15 @@
     for i in range(4):
         arrived(("a1l", i), a_r1.at[i, 0])
         f_sum[4 + i, yr, :, 0:32] = (f_sum[4 + i, yr, :, 0:32].astype(F32) + a_r1[i, 0].astype(F32)).astype(BF16)
-        send(("a2l", i), f_sum.at[4 + i, yr], a_r2.at[i, 0], y_right)
+        send(("a2l", i), f_sum.at[4 + i, yr], a_r2.at[i, 0], y_right, ("a2", i))
         arrived(("a1r", i), a_r1.at[i, 1])
         f_sum[4 + i, yl, :, 32:64] = (f_sum[4 + i, yl, :, 32:64].astype(F32) + a_r1[i, 1].astype(F32)).astype(BF16)
-        send(("a2r", i), f_sum.at[4 + i, yl], a_r2.at[i, 1], y_left)
+        send(("a2r", i), f_sum.at[4 + i, yl], a_r2.at[i, 1], y_left, ("a2", i))
     z_own_forward("gu")
     z_pass("gu", "q")
     square = jnp.zeros((ROWS, 1), F32)
     for i in range(4):
-        arrived(("a2l", i), a_r2.at[i, 0])
-        arrived(("a2r", i), a_r2.at[i, 1])
+        arrived(("a2", i), a_r2.at[i])
         for n in range(2):
             cols = cols_of(2 * i + n)
             s = part[i, y, n, c].astype(F32) + a_d2d[i, y, n].astype(F32)
@@ -438,9 +460,6 @@
     z_far_other("gu")
     x_pass("gu", "o", "p", "q", "o")
     x_own("d", "o")
-    z_other_forward("d")
-    for turn in ("l", "r"):
-        x_pass("d", turn, "p", "q")
     ring_forward(1, oh)
     from_core(1, yl)
     from_core(2, yr)
@@ -451,6 +470,7 @@
 
     ring_last(0, h)
     z_pass_forward("gu", "o")
+    z_other("d")
     z_own("d")
     z_pass("d", "p")
     z_pass("d", "q")
@@ -525,10 +545,10 @@
     def sum_far(i):
         arrived(("f1l", i), f_r1.at[i, 0])
         f_sum[i, yr, :, 0:32] = (f_sum[i, yr, :, 0:32].astype(F32) + f_r1[i, 0].astype(F32)).astype(BF16)
-        send(("f2l", i), f_sum.at[i, yr], f_r2.at[i, 0], y_right)
+        send(("f2l", i), f_sum.at[i, yr], f_r2.at[i, 0], y_right, ("f2", i))
         arrived(("f1r", i), f_r1.at[i, 1])
         f_sum[i, yl, :, 32:64] = (f_sum[i, yl, :, 32:64].astype(F32) + f_r1[i, 1].astype(F32)).astype(BF16)
-        send(("f2r", i), f_sum.at[i, yl], f_r2.at[i, 1], y_left)
+        send(("f2r", i), f_sum.at[i, yl], f_r2.at[i, 1], y_left, ("f2", i))
 
     def ring_sum(i, pp):
         return f_sum[i, y, pp].astype(F32) + f_r2[i, 0, pp].astype(F32) + f_r2[i, 1, pp].astype(F32)
@@ -536,8 +556,7 @@
     def sum_near(i):
         if i >= 2:
             drain(("f1l", i - 1), ("f1r", i - 1), ("f2l", i - 2), ("f2r", i - 2), ("fx", i - 2))
-        arrived(("f2l", i), f_r2.at[i, 0])
-        arrived(("f2r", i), f_r2.at[i, 1])
+        arrived(("f2", i), f_r2.at[i])
         f_sum[i, y, oh] = ring_sum(i, oh).astype(BF16)
         send(("fx", i), f_sum.at[i, y, oh], f_xr.at[i], x_pair)
 
@@ -547,6 +566,9 @@
         cols = pl.ds(pl.multiple_of(zz * 1024 + j * CH, CH), CH)
         out_ref[:, cols] = (stream[:, cols] + 0.5 * (ring_sum(i, h) + f_xr[i].astype(F32))).astype(BF16)
 
+    z_other_forward("d")
+    for turn in ("l", "r"):
+        x_pass("d", turn, "p", "q")
     down(0)
     z_pass("d", "o")
     down(1)
@@ -554,53 +576,52 @@
     z_own_forward("d")
     for turn in ("l", "r"):
         x_pass("d", turn, "o")
-    z_far_other("d")
-    x_pass("d", "o", "p", "q")
     sum_cores(1)
     sum_far(0)
     z_pass_forward("d", "p")
+    sum_far(1)
     x_done("d", "l", "p")
     down(2)
     x_done("d", "r", "p")
     down(3)
-    sum_far(1)
+    sum_near(0)
     sum_cores(2)
-    sum_near(0)
+    z_pass_forward("d", "q")
     sum_cores(3)
-    z_pass_forward("d", "q")
-    sum_near(1)
+    z_far_other("d")
+    x_pass("d", "o", "p", "q")
     sum_far(2)
     z_pass_forward("d", "o")
     x_done("d", "l", "q", "o")
     down(4)
+    sum_far(3)
     x_done("d", "r", "q", "o")
     down(5)
-    sum_far(3)
+    sum_near(1)
     z_far_own("d")
     x_pass("d", "o", "o")
     sum_cores(4)
     sum_cores(5)
-    sum_near(2)
     drain(("x", "d"), ("z", "d"), ("f", "gu"), ("xb", "d", "l"), ("xb", "d", "r"), ("f", "d", "s"))
     z_done("d", "p")
     x_done("d", "o", "p")
     down(6)
     sum_far(4)
-    sum_near(3)
+    sum_near(2)
     sum_cores(6)
     z_done("d", "q", "o")
     x_done("d", "o", "q", "o")
     down(7)
     sum_far(5)
+    sum_near(3)
+    sum_cores(7)
+    sum_far(6)
     sum_near(4)
-    sum_cores(7)
+    sum_far(7)
     finish(0)
-    sum_far(6)
     finish(1)
     sum_near(5)
-    finish(2)
-    sum_far(7)
-    for i in range(3, 6):
+    for i in range(2, 6):
         finish(i)
     sum_near(6)
     sum_near(7)
@@ -619,6 +640,15 @@
     vmem = pl.BlockSpec(memory_space=pltpu.VMEM)
     anywhere = pl.BlockSpec(memory_space=pl.ANY)
     scratch = [
+        pltpu.VMEM((TOK, 128), BF16),
+        pltpu.VMEM((TOK, 128), BF16),
+        pltpu.VMEM((TOK, 256), BF16),
+        pltpu.VMEM((TOK, 256), BF16),
+        pltpu.VMEM((2, TOK), F32),
+        pltpu.VMEM((2, TOK), F32),
+        pltpu.VMEM((2, TOK), F32),
+        pltpu.VMEM((256,), BF16),
+        pltpu.VMEM((D,), BF16),
         pltpu.VMEM((16, 256, WIDE), BF16),
         pltpu.VMEM((16, 256, PADDED), BF16),
         pltpu.VMEM((256, WIDE), BF16),
@@ -642,23 +672,23 @@
         pltpu.VMEM((8, 2, 2, 32, CH), BF16),
         pltpu.VMEM((8, 2, 2, ROWS, CH), BF16),
         pltpu.VMEM((8, ROWS, CH), BF16),
-        pltpu.VMEM((4, 128, 128), BF16),
+        pltpu.VMEM((4, 128, 128), F32),
         pltpu.VMEM((4, 8, 128), F32),
-        pltpu.VMEM((4, 128, 128), BF16),
+        pltpu.VMEM((4, 128, 128), F32),
         pltpu.VMEM((4, 8, 128), F32),
         pltpu.VMEM((2, TOK, 128), F32),
         pltpu.VMEM((2, TOK, 2), F32),
         pltpu.VMEM((8, TOK), F32),
-        pltpu.SemaphoreType.DMA((NSEM,)),
+        pltpu.SemaphoreType.DMA((NSEND,)),
         pltpu.SemaphoreType.DMA((NSEM,)),
         pltpu.SemaphoreType.DMA((2, 4)),
         pltpu.SemaphoreType.DMA((2, 4)),
-        pltpu.SemaphoreType.DMA((12,)),
+        pltpu.SemaphoreType.DMA((21,)),
     ]
     return pl.pallas_call(
         kernel,
         out_shape=jax.ShapeDtypeStruct((ROWS, D), BF16),
-        in_specs=[vmem] * 9 + [anywhere] * 5,
+        in_specs=[anywhere] * 14,
         out_specs=vmem,
         scratch_shapes=scratch,
         compiler_params=pltpu.CompilerParams(

time: 155 us -> 153 us (0.987)
  Pallas kernels: 153 us -> 150 us
    pallas_call x1, Pallas kernels: 153 us -> 150 us  [per_device(): pl.pallas_call(kernel, out_shape=jax.ShapeDtypeStruct((ROWS, D), BF16), i...]
where the time goes in v2:
time: 153 us; the launch traced here: 151 us
  Pallas kernels  150 us (98%)
  local copies, waits for them, and re-layouts  1.87 us (1%)
    pallas_call x1, Pallas kernels, per_device(): pl.pallas_call(kernel, out_shape=jax.ShapeDtypeStruct((ROWS, D), BF16), i...  150 us

profile of v2, /device:TPU:0, one launch (start us, length us, event | category | flops | bytes accessed | tf_op | source)
XLA Modules:
  0.0 151.5 jit_solution(14756897423416798350)
XLA Ops:
  0.0 149.6 %layer.1 = bf16[64,4096]{1,0:T(8,128)(2,1)} custom-call(bf16[512,128]{1,0:T(8,128)(2,1)} %q_hbm.1, bf16[512,128]{1,0:T(8,128)(2,1)} %k_hbm.1, bf16[512,256]{1,0:T(8,128)(2,1)} %v_hbm.1, bf16[512,256]{1,0:T(8,128)(2,1)} %og_hbm.1, f32[2,512]{1,0:T(2,128)} %ig_hbm.1, f32[2,512]{1,0:T(2,128)} %fl_hbm.1, f32[2,512]{1,0:T(2,128)} %ef_hbm.1, ...), custom_call_target="tpu_custom_call" | custom-call | tf_op jit(solution)/shard_map/layer/pallas_call | solution.py:688
  149.6 1.9 %copy.16 = bf16[64,4096]{1,0:T(8,128)(2,1)} copy(bf16[64,4096]{1,0:T(8,128)(2,1)} %layer.1) | data formatting | bytes 1048576
